TPU v7x, 32 devices: a whole 2x2x4 slice. The times are simulated.
32 devices in a mesh: ep: 32 (over z, y, x, core).
Axes of the slice: x: 2, y: 2, z: 4, core: 2. Of those that a mesh axis runs over, the one named last changes fastest.
Arguments:
- tokens: bfloat16 [512, 2048], P('ep'), may hold values from -6 to 6
- cache_keys: bfloat16 [512, 1024, 128], P('ep'), may hold values from -6 to 6
- cache_values: bfloat16 [512, 1024, 128], P('ep'), may hold values from -6 to 6
- cache_len: int32 [512], P('ep'), may hold values from 1 to 1024
- norm_gain_first: float32 [2048], replicated, may hold values from 0.1 to 1.9
- w_query: bfloat16 [2048, 2048], P(None, 'ep'), may hold values from -0.125 to 0.125
- w_key: bfloat16 [2048, 128], replicated, may hold values from -0.125 to 0.125
- w_value: bfloat16 [2048, 128], replicated, may hold values from -0.125 to 0.125
- head_bias: float32 [32], replicated, may hold values from -8.5 to -3
- w_output: bfloat16 [2048, 2048], P(None, 'ep'), may hold values from -0.125 to 0.125
- norm_gain_second: float32 [2048], replicated, may hold values from 0.1 to 1.9
- group_id: int32 [512], P('ep'), may hold values from 0 to 1, as said below
- member: int32 [512, 6], P('ep'), may hold values from 0 to 15, as said below
- group_gate: float32 [512], P('ep'), may hold values from 0.3 to 1
- member_weight: float32 [512, 6], P('ep'), may hold values from 0.05 to 0.5
- expert_gate_w: bfloat16 [32, 2048, 512], P('ep'), may hold values from -0.125 to 0.125
- expert_up_w: bfloat16 [32, 2048, 512], P('ep'), may hold values from -0.125 to 0.125
- expert_down_w: bfloat16 [32, 512, 2048], P('ep'), may hold values from -0.25 to 0.25
- dense_gate_w: bfloat16 [2048, 2048], P(None, 'ep'), may hold values from -0.125 to 0.125
- dense_up_w: bfloat16 [2048, 2048], P(None, 'ep'), may hold values from -1 to 1
- hidden_gain: float32 [2048], replicated, may hold values from 0.1 to 1.9
- dense_down_w: bfloat16 [2048, 2048], P(None, 'ep'), may hold values from -0.125 to 0.125
- branch_logit: float32 [2048], replicated, may hold values from -8 to 8
Outputs:
- mixed_out: bfloat16 [512, 2048], P('ep')
- new_keys: bfloat16 [512, 128], P('ep')
- new_values: bfloat16 [512, 128], P('ep')
Inputs may be any that keep to these rules, and one draw needn't show every extreme that they name: `group_id`: each group number is named by exactly 8 of the tokens of one device. `member`: each row names 6 different members; with group_id, no expert is named by more than 8 tokens of one device, and some expert is named by 8 tokens of every device.
All inputs are finite; a program needn't handle non-finite values.
Results may differ from a plain program's by a relative error of at most 0.0085.
Values may be sent and summed in bfloat16 or wider, within the bound.
A program may use at most 128 MiB of HBM per device.

v0:
```python
import functools

import jax
import jax.numpy as jnp
from jax import lax
from jax.experimental import pallas as pl
from jax.experimental.pallas import tpu as pltpu
from jax.sharding import PartitionSpec as P

HEADS = 32
HEAD_DIM = 64
KV_HEADS = 2
PER_GROUP = 16
TOP_K = 6
LANES = 128
MESH = pl.DeviceIdType.MESH

epsilon = 1e-06


def torus_of(chips):
    best = (chips, 1, 1)
    for x in range(1, chips + 1):
        for y in range(x, chips + 1):
            if chips % (x * y) == 0 and chips // (x * y) >= y:
                z = chips // (x * y)
                if z + y + x < sum(best):
                    best = (z, y, x)
    return best


def rms_scale(values):
    return lax.rsqrt(jnp.mean(values * values, axis=-1, keepdims=True) + epsilon)


class Place:
    def __init__(self, chips):
        self.chips = chips
        self.dims = torus_of(chips)
        me = lax.axis_index("ep")
        self.core = lax.rem(me, 2)
        self.chip = me // 2
        depth, height, width = self.dims
        self.x = lax.rem(self.chip, width)
        self.y = lax.rem(self.chip // width, height)
        self.z = self.chip // (width * height)

    def at(self, dz, dy, dx):
        depth, height, width = self.dims
        z = lax.rem(self.z + dz + depth, depth)
        y = lax.rem(self.y + dy + height, height)
        x = lax.rem(self.x + dx + width, width)
        return (z * height + y) * width + x

    def device(self, chip):
        return (chip * 2 + self.core,)

    def greet(self):
        barrier = pltpu.get_barrier_semaphore()
        for step in range(1, self.chips):
            other = lax.rem(self.chip + step, self.chips)
            pl.semaphore_signal(barrier, inc=1, device_id=self.device(other), device_id_type=MESH)
        pl.semaphore_wait(barrier, self.chips - 1)


def spread(place, halves):
    depth, height, width = place.dims
    sent = []
    counts = [0, 0]

    def push(half, source, origin, target):
        own, slots, send, recv = halves[half]
        copy = pltpu.make_async_remote_copy(
            src_ref=own if source is None else slots.at[source],
            dst_ref=slots.at[origin],
            send_sem=send.at[counts[half]],
            recv_sem=recv.at[origin],
            device_id=place.device(target),
            device_id_type=MESH,
        )
        counts[half] += 1
        copy.start()
        sent.append(copy)

    def arrive(half, origin):
        own, slots, send, recv = halves[half]
        pltpu.make_async_remote_copy(
            src_ref=slots.at[origin],
            dst_ref=slots.at[origin],
            send_sem=send.at[0],
            recv_sem=recv.at[origin],
            device_id=place.device(place.chip),
            device_id_type=MESH,
        ).wait_recv()

    def along(half, source, origin, axis):
        if axis == "x":
            for step in range(1, width):
                push(half, source, origin, place.at(0, 0, step))
        else:
            for step in range(1, height):
                push(half, source, origin, place.at(0, step, 0))

    orders = (("x", "y"), ("y", "x"))
    for step in range(1, depth):
        for half in range(2):
            push(half, None, place.chip, place.at(step, 0, 0))
    for half in range(2):
        for axis in orders[half]:
            along(half, None, place.chip, axis)
    for step in range(1, depth):
        for half in range(2):
            origin = place.at(-step, 0, 0)
            arrive(half, origin)
            for axis in orders[half]:
                along(half, origin, origin, axis)
    for up in range(depth):
        for half in range(2):
            reach = width if half == 0 else height
            for step in range(1, reach):
                origin = place.at(-up, 0, -step) if half == 0 else place.at(-up, -step, 0)
                arrive(half, origin)
                along(half, origin, origin, orders[half][1])
    for up in range(depth):
        for half in range(2):
            for dy in range(height):
                for dx in range(width):
                    if (dy if half == 0 else dx) != 0:
                        arrive(half, place.at(-up, -dy, -dx))
    for half in range(2):
        own, slots, _, _ = halves[half]
        slots[place.chip] = own[...]
    return sent


def deliver(place, tiles, landed, send, recv, out_ref):
    copies = []
    for step in range(1, place.chips):
        other = lax.rem(place.chip + step, place.chips)
        copy = pltpu.make_async_remote_copy(
            src_ref=tiles.at[other],
            dst_ref=landed.at[place.chip],
            send_sem=send.at[step],
            recv_sem=recv.at[place.chip],
            device_id=place.device(other),
            device_id_type=MESH,
        )
        copy.start()
        copies.append(copy)
    landed[place.chip] = tiles[place.chip]
    for step in range(1, place.chips):
        origin = lax.rem(place.chip - step + place.chips, place.chips)
        pltpu.make_async_remote_copy(
            src_ref=landed.at[origin],
            dst_ref=landed.at[origin],
            send_sem=send.at[0],
            recv_sem=recv.at[origin],
            device_id=place.device(place.chip),
            device_id_type=MESH,
        ).wait_recv()
    lanes = landed.shape[2]
    for block in range(place.chips):
        out_ref[:, block * lanes : (block + 1) * lanes] = landed[block]
    for copy in copies:
        copy.wait_send()


def flat(slots):
    count, rows, columns = slots.shape
    return slots[...].reshape(count * rows, columns)


def project_kernel(chips, a_ref, b_ref, w_ref, out_ref, slots_a, slots_b, tiles, landed,
                   send_a, recv_a, send_b, recv_b, send_t, recv_t):
    place = Place(chips)
    place.greet()
    sent = spread(place, ((a_ref, slots_a, send_a, recv_a), (b_ref, slots_b, send_b, recv_b)))
    cut = a_ref.shape[1]
    product = jnp.dot(flat(slots_a), w_ref[:cut], preferred_element_type=jnp.float32)
    product = product + jnp.dot(flat(slots_b), w_ref[cut:], preferred_element_type=jnp.float32)
    tiles[...] = product.astype(jnp.bfloat16).reshape(tiles.shape)
    deliver(place, tiles, landed, send_t, recv_t, out_ref)
    for copy in sent:
        copy.wait_send()


def gather_kernel(chips, a_ref, b_ref, gate_ref, up_ref, rows_ref, notes_ref, hidden_ref, slots_a, slots_b,
                  send_a, recv_a, send_b, recv_b):
    place = Place(chips)
    place.greet()
    sent = spread(place, ((a_ref, slots_a, send_a, recv_a), (b_ref, slots_b, send_b, recv_b)))
    cut = b_ref.shape[1]
    rows_a = slots_a[:, :, :cut].reshape(chips * a_ref.shape[0], cut)
    rows_b = flat(slots_b)
    rows_ref[:, :cut] = rows_a
    rows_ref[:, cut:] = rows_b
    notes_ref[...] = slots_a[:, :, cut:].reshape(notes_ref.shape)
    gate = jnp.dot(rows_a, gate_ref[:cut], preferred_element_type=jnp.float32)
    gate = gate + jnp.dot(rows_b, gate_ref[cut:], preferred_element_type=jnp.float32)
    upper = jnp.dot(rows_a, up_ref[:cut], preferred_element_type=jnp.float32)
    upper = upper + jnp.dot(rows_b, up_ref[cut:], preferred_element_type=jnp.float32)
    hidden_ref[...] = (jax.nn.silu(gate) * upper).astype(jnp.bfloat16)
    for copy in sent:
        copy.wait_send()


def down_kernel(chips, a_ref, b_ref, gain_ref, w_ref, out_ref, slots_a, slots_b, tiles, landed,
                send_a, recv_a, send_b, recv_b, send_t, recv_t):
    place = Place(chips)
    place.greet()
    sent = spread(place, ((a_ref, slots_a, send_a, recv_a), (b_ref, slots_b, send_b, recv_b)))
    rows, lanes = a_ref.shape
    part = chips // 2
    for half, slots in enumerate((slots_a, slots_b)):
        square = jnp.zeros((rows, lanes), jnp.float32)
        for block in range(chips):
            value = slots[block].astype(jnp.float32)
            square = square + value * value
        mean = jnp.sum(square, axis=1, keepdims=True) / (chips * lanes)
        scale = lax.rsqrt(mean + epsilon)
        total = jnp.zeros((rows, lanes), jnp.float32)
        for block in range(chips):
            gain = gain_ref[:, block * lanes : (block + 1) * lanes]
            normed = (slots[block].astype(jnp.float32) * scale * gain).astype(jnp.bfloat16)
            total = total + jnp.dot(
                normed,
                w_ref[block * lanes : (block + 1) * lanes],
                preferred_element_type=jnp.float32,
            )
        tiles[half * part : (half + 1) * part] = total.astype(jnp.bfloat16).reshape(
            part, rows // part, lanes
        )
    deliver(place, tiles, landed, send_t, recv_t, out_ref)
    for copy in sent:
        copy.wait_send()


def whole():
    return pl.BlockSpec(memory_space=pltpu.VMEM)


def spread_scratch(chips, a, b):
    slots = [pltpu.VMEM((chips,) + a.shape, a.dtype), pltpu.VMEM((chips,) + b.shape, b.dtype)]
    return slots, [pltpu.SemaphoreType.DMA((chips,))] * 4


def remote_params(number):
    return pltpu.CompilerParams(collective_id=number, has_side_effects=True)


def project(chips, number, rows, weight):
    count, width = rows.shape
    lanes = weight.shape[1]
    a, b = rows[:, : width // 2], rows[:, width // 2 :]
    slots, sems = spread_scratch(chips, a, b)
    tile = pltpu.VMEM((chips, count, lanes), jnp.bfloat16)
    return pl.pallas_call(
        functools.partial(project_kernel, chips),
        out_shape=jax.ShapeDtypeStruct((count, chips * lanes), jnp.bfloat16),
        in_specs=[whole()] * 3,
        out_specs=whole(),
        scratch_shapes=slots + [tile, tile] + sems + [pltpu.SemaphoreType.DMA((chips,))] * 2,
        compiler_params=remote_params(number),
        name="project",
    )(a, b, weight)


def gather_rows(chips, number, rows, notes, gate_w, up_w):
    count, width = rows.shape
    a = jnp.concatenate([rows[:, : width // 2], notes], axis=1)
    b = rows[:, width // 2 :]
    slots, sems = spread_scratch(chips, a, b)
    return pl.pallas_call(
        functools.partial(gather_kernel, chips),
        out_shape=(
            jax.ShapeDtypeStruct((chips * count, width), jnp.bfloat16),
            jax.ShapeDtypeStruct((chips * count, LANES), jnp.bfloat16),
            jax.ShapeDtypeStruct((chips * count, gate_w.shape[1]), jnp.bfloat16),
        ),
        in_specs=[whole()] * 4,
        out_specs=(whole(),) * 3,
        scratch_shapes=slots + sems,
        compiler_params=remote_params(number),
        name="gather_rows",
    )(a, b, gate_w, up_w)


def down_project(chips, number, hidden, gain, weight):
    count, lanes = hidden.shape
    a, b = hidden[: count // 2], hidden[count // 2 :]
    slots, sems = spread_scratch(chips, a, b)
    tile = pltpu.VMEM((chips, count // chips, lanes), jnp.bfloat16)
    return pl.pallas_call(
        functools.partial(down_kernel, chips),
        out_shape=jax.ShapeDtypeStruct((count // chips, chips * lanes), jnp.bfloat16),
        in_specs=[whole()] * 4,
        out_specs=whole(),
        scratch_shapes=slots + [tile, tile] + sems + [pltpu.SemaphoreType.DMA((chips,))] * 2,
        compiler_params=remote_params(number),
        name="down_project",
    )(a, b, gain[None, :], weight)


def stick_kernel(lens_ref, q_ref, k_ref, v_ref, bias_ref, out_ref):
    step = pl.program_id(0)
    batch, span, _ = k_ref.shape
    blocks = span // LANES
    row = lax.broadcasted_iota(jnp.int32, (3 * LANES, LANES), 0)
    column = lax.broadcasted_iota(jnp.int32, (3 * LANES, LANES), 1)
    after = (lax.rem(row, LANES) > column).astype(jnp.bfloat16)
    place = lax.broadcasted_iota(jnp.int32, (HEADS, span), 1)
    bias = bias_ref[:, :1]
    group = HEADS // KV_HEADS
    head = lax.broadcasted_iota(jnp.int32, (HEADS, LANES), 0)
    lane = lax.broadcasted_iota(jnp.int32, (HEADS, LANES), 1)
    own_lanes = (head // group) == (lane // HEAD_DIM)
    late = lax.broadcasted_iota(jnp.int32, (HEADS, HEAD_DIM), 0) >= group
    for item in range(batch):
        heads = q_ref[item].astype(jnp.float32)
        heads = jnp.where(own_lanes, jnp.concatenate([heads] * KV_HEADS, axis=1), 0.0)
        scores = lax.dot_general(
            heads.astype(jnp.bfloat16), k_ref[item], (((1,), (1,)), ((), ())), preferred_element_type=jnp.float32
        )
        scores = scores * HEAD_DIM ** (-0.5) + bias
        live = place < lens_ref[step * batch + item]
        remain = -(jnp.maximum(scores, 0.0) + jnp.log1p(jnp.exp(-jnp.abs(scores))))
        log_remain = jnp.where(live, remain, 0.0)
        stacked = jnp.concatenate(
            [log_remain[:, n * LANES : (n + 1) * LANES] for n in range(blocks)], axis=0
        )
        high = stacked.astype(jnp.bfloat16)
        rest = stacked - high.astype(jnp.float32)
        middle = rest.astype(jnp.bfloat16)
        low = (rest - middle.astype(jnp.float32)).astype(jnp.bfloat16)
        within = jnp.dot(
            jnp.concatenate([high, middle, low], axis=1), after, preferred_element_type=jnp.float32
        )
        totals = jnp.sum(stacked, axis=1, keepdims=True)
        carried = jnp.zeros((HEADS, 1), jnp.float32)
        pieces = [None] * blocks
        for n in range(blocks - 1, -1, -1):
            pieces[n] = within[n * HEADS : (n + 1) * HEADS] + carried
            carried = carried + totals[n * HEADS : (n + 1) * HEADS]
        remain_after = jnp.concatenate(pieces, axis=1)
        weights = jnp.where(live, jnp.exp(scores + remain + remain_after), 0.0)
        mixed = jnp.dot(
            weights.astype(jnp.bfloat16), v_ref[item], preferred_element_type=jnp.float32
        )
        mixed = jnp.where(late, mixed[:, HEAD_DIM:], mixed[:, :HEAD_DIM])
        out_ref[item] = mixed.astype(jnp.bfloat16)


def stick_read(queries, key_cache, value_cache, lengths, head_bias):
    batch, span, lanes = key_cache.shape
    heads = queries.reshape(batch, HEADS, HEAD_DIM)
    each = min(4, batch)
    mixed = pl.pallas_call(
        stick_kernel,
        out_shape=jax.ShapeDtypeStruct((batch, HEADS, HEAD_DIM), jnp.bfloat16),
        grid=(batch // each,),
        in_specs=[
            pl.BlockSpec(memory_space=pltpu.SMEM),
            pl.BlockSpec((each, HEADS, HEAD_DIM), lambda i: (i, 0, 0)),
            pl.BlockSpec((each, span, lanes), lambda i: (i, 0, 0)),
            pl.BlockSpec((each, span, lanes), lambda i: (i, 0, 0)),
            pl.BlockSpec((HEADS, LANES), lambda i: (0, 0)),
        ],
        out_specs=pl.BlockSpec((each, HEADS, HEAD_DIM), lambda i: (i, 0, 0)),
        name="stick_read",
    )(lengths, heads, key_cache, value_cache, jnp.broadcast_to(head_bias[:, None], (HEADS, LANES)))
    return mixed.reshape(batch, HEADS * HEAD_DIM)


def shards(
    tokens,
    cache_keys,
    cache_values,
    cache_len,
    norm_gain_first,
    w_query,
    w_key,
    w_value,
    head_bias,
    w_output,
    norm_gain_second,
    group_id,
    member,
    group_gate,
    member_weight,
    expert_gate_w,
    expert_up_w,
    expert_down_w,
    dense_gate_w,
    dense_up_w,
    hidden_gain,
    dense_down_w,
    branch_logit,
):
    devices = lax.axis_size("ep")
    chips = devices // 2
    me = lax.axis_index("ep")
    first = lax.rem(me, 2) == 0
    partner = [(i, i + 1 - 2 * (i % 2)) for i in range(devices)]
    seq_dev, width = tokens.shape

    def both(own):
        other = lax.ppermute(own, "ep", partner)
        return jnp.where(
            first, jnp.concatenate([own, other], axis=-1), jnp.concatenate([other, own], axis=-1)
        )

    query_w = both(w_query)
    output_w = both(w_output)
    gate_w = both(dense_gate_w)
    up_w = both(dense_up_w)
    down_w = both(dense_down_w)

    stream = tokens.astype(jnp.float32)
    normed_first = (stream * rms_scale(stream) * norm_gain_first).astype(jnp.bfloat16)
    new_keys = jnp.dot(normed_first, w_key, preferred_element_type=jnp.float32).astype(jnp.bfloat16)
    new_values = jnp.dot(normed_first, w_value, preferred_element_type=jnp.float32).astype(
        jnp.bfloat16
    )
    queries = project(chips, 1, normed_first, query_w)
    attended = stick_read(queries, cache_keys, cache_values, cache_len, head_bias)
    projected = project(chips, 2, attended, output_w)
    second_stream = stream + projected.astype(jnp.float32)
    normed_second = (second_stream * rms_scale(second_stream) * norm_gain_second).astype(
        jnp.bfloat16
    )

    experts = devices * expert_gate_w.shape[0]
    capacity = seq_dev // (experts // PER_GROUP)
    notes = jnp.concatenate(
        [member, group_id[:, None], jnp.zeros((seq_dev, LANES - TOP_K - 1), jnp.int32)], axis=1
    ).astype(jnp.bfloat16)
    own_rows, own_notes, hidden = gather_rows(chips, 3, normed_second, notes, gate_w, up_w)
    other_rows = lax.ppermute(own_rows, "ep", partner)
    other_notes = lax.ppermute(own_notes, "ep", partner)
    dense_out = down_project(chips, 4, hidden, hidden_gain, down_w)

    def selection(rows_notes, parity):
        table = rows_notes[:, : TOP_K + 1].astype(jnp.int32)
        named = table[:, TOP_K :] * PER_GROUP + table[:, :TOP_K]
        hits = jnp.any(named == me, axis=1).reshape(chips, seq_dev)
        index = jnp.arange(seq_dev)
        earlier = (index[:, None] < index[None, :]).astype(jnp.float32)
        slot = jnp.dot(hits.astype(jnp.float32), earlier).astype(jnp.int32)
        spot = ((jnp.arange(chips)[:, None] * 2 + parity) * capacity + slot).reshape(-1)
        spot = jnp.where(hits.reshape(-1), spot, -1)
        return (jnp.arange(devices * capacity)[:, None] == spot[None, :]).astype(jnp.bfloat16)

    parity = lax.rem(me, 2)
    packed = jnp.dot(selection(own_notes, parity), own_rows, preferred_element_type=jnp.float32)
    packed = packed + jnp.dot(
        selection(other_notes, 1 - parity), other_rows, preferred_element_type=jnp.float32
    )
    packed = packed.astype(jnp.bfloat16)
    gate_pre = jnp.dot(packed, expert_gate_w[0], preferred_element_type=jnp.float32)
    upper_pre = jnp.dot(packed, expert_up_w[0], preferred_element_type=jnp.float32)
    expert_hidden = (jax.nn.silu(gate_pre) * upper_pre).astype(jnp.bfloat16)
    served = jnp.dot(expert_hidden, expert_down_w[0], preferred_element_type=jnp.float32).astype(
        jnp.bfloat16
    )
    returned = lax.all_to_all(
        served.reshape(devices, capacity, width), "ep", split_axis=0, concat_axis=0, tiled=True
    ).reshape(experts * capacity, width)

    pair_expert = (group_id[:, None] * PER_GROUP + member).reshape(-1)
    pair_count = pair_expert.shape[0]
    expert_hits = (pair_expert[:, None] == jnp.arange(experts, dtype=jnp.int32)[None, :]).astype(
        jnp.float32
    )
    earlier = (jnp.arange(pair_count)[:, None] > jnp.arange(pair_count)[None, :]).astype(
        jnp.float32
    )
    before = jnp.dot(earlier, expert_hits, preferred_element_type=jnp.float32)
    slot_index = jnp.sum(before * expert_hits, axis=1).astype(jnp.int32)
    target = pair_expert * capacity + slot_index
    select = (target[:, None] == jnp.arange(experts * capacity, dtype=jnp.int32)[None, :]).astype(
        jnp.bfloat16
    )
    pair_out = jnp.dot(select, returned, preferred_element_type=jnp.float32)
    combine = (group_gate[:, None] * member_weight).reshape(-1, 1)
    routed = jnp.sum((pair_out * combine).reshape(seq_dev, TOP_K, width), axis=1)
    mixed_out = (
        second_stream + routed + jax.nn.sigmoid(branch_logit) * dense_out.astype(jnp.float32)
    )
    return (mixed_out.astype(jnp.bfloat16), new_keys, new_values)


def solution(mesh):
    in_specs = (
        P("ep", None),
        P("ep", None, None),
        P("ep", None, None),
        P("ep"),
        P(),
        P(None, "ep"),
        P(),
        P(),
        P(),
        P(None, "ep"),
        P(),
        P("ep"),
        P("ep", None),
        P("ep"),
        P("ep", None),
        P("ep", None, None),
        P("ep", None, None),
        P("ep", None, None),
        P(None, "ep"),
        P(None, "ep"),
        P(),
        P(None, "ep"),
        P(),
    )
    out_specs = (P("ep", None), P("ep", None), P("ep", None))
    return jax.shard_map(shards, mesh=mesh, in_specs=in_specs, out_specs=out_specs, check_vma=False)
```

profile of v0, /device:TPU:0, one launch (start us, length us, event | category | flops | bytes accessed | tf_op | source)
XLA Modules:
  0.0 173.5 jit_solution(8889830614820188981)
XLA Ops:
  0.7 1.4 copy.96
  2.6 1.2 copy.93
  4.0 2.0 %copy.87 = bf16[2048,64]{1,0:T(8,128)(2,1)} copy(bf16[2048,64]{0,1:T(8,128)(2,1)} %param.32) | data formatting | bytes 524288 | tf_op args[9]
  8.6 1.1 collective-permute-done
  9.7 2.9 %maximum_select_fusion.w_ref = bf16[2048,128]{1,0:T(8,128)(2,1)} fusion(bf16[2048,64]{1,0:T(8,128)(2,1)} %collective-permute-done, bf16[2048,64]{1,0:T(8,128)(2,1)} %copy.84, pred[]{:T(512)S(6)} %eq.32), kind=kLoop, calls=%fused_computation.21 | loop fusion | flops 2359296 | bytes 1048577 | tf_op jit(solution)/shard_map/jit(_where)/select_n | solution.py:408
  12.6 28.6 %project.2 = bf16[16,2048]{1,0:T(8,128)(2,1)} custom-call(bf16[16,1024]{1,0:T(8,128)(2,1)} %get-tuple-element.16.a_ref, bf16[16,1024]{1,0:T(8,128)(2,1)} %get-tuple-element.15.b_ref, bf16[2048,128]{1,0:T(8,128)(2,1)} %maximum_select_fusion.w_ref), custom_call_target="tpu_custom_call" | custom-call | tf_op jit(solution)/shard_map/project/pallas_call | solution.py:257
  41.2 1.7 reshape.99.q_ref
  43.6 9.8 %stick_read.1 = bf16[16,32,64]{2,1,0:T(8,128)(2,1)} custom-call(s32[16]{0:T(128)} %lens_ref.1, bf16[16,32,64]{2,1,0:T(8,128)(2,1)} %reshape.99.q_ref, bf16[16,1024,128]{2,1,0:T(8,128)(2,1)} %k_ref.1, bf16[16,1024,128]{2,1,0:T(8,128)(2,1)} %v_ref.1, f32[32,128]{1,0:T(8,128)} %broadcast_in_dim.13.bias_ref), custom_call_target="tpu_custom_call" | custom-call | tf_op jit(solution)/shard_map/stick_read/pallas_call | solution.py:357
  55.1 3.0 %maximum_select_fusion.1.w_ref = bf16[2048,128]{1,0:T(8,128)(2,1)} fusion(bf16[2048,64]{1,0:T(8,128)(2,1)} %collective-permute-done.1, bf16[2048,64]{1,0:T(8,128)(2,1)} %copy.87, pred[]{:T(512)S(6)} %eq.32), kind=kLoop, calls=%fused_computation.22 | loop fusion | flops 2359296 | bytes 1048577 | tf_op jit(solution)/shard_map/jit(_where)/select_n | solution.py:408
  58.1 21.5 %project.3 = bf16[16,2048]{1,0:T(8,128)(2,1)} custom-call(bf16[16,1024]{1,0:T(8,128)(2,1)} %get-tuple-element.14.a_ref, bf16[16,1024]{1,0:T(8,128)(2,1)} %get-tuple-element.13.b_ref, bf16[2048,128]{1,0:T(8,128)(2,1)} %maximum_select_fusion.1.w_ref), custom_call_target="tpu_custom_call" | custom-call | tf_op jit(solution)/shard_map/project/pallas_call | solution.py:257
  82.8 2.6 %maximum_select_fusion.3.up_ref = bf16[2048,128]{1,0:T(8,128)(2,1)} fusion(bf16[2048,64]{1,0:T(8,128)(2,1)} %collective-permute-done.3, bf16[2048,64]{1,0:T(8,128)(2,1)S(1)} %copy.96, pred[]{:T(512)S(6)} %eq.32), kind=kLoop, calls=%fused_computation.24 | loop fusion | flops 2359296 | bytes 1048577 | tf_op jit(solution)/shard_map/jit(_where)/select_n | solution.py:408
  85.5 2.6 %maximum_select_fusion.2.gate_ref = bf16[2048,128]{1,0:T(8,128)(2,1)} fusion(bf16[2048,64]{1,0:T(8,128)(2,1)} %collective-permute-done.2, bf16[2048,64]{1,0:T(8,128)(2,1)S(1)} %copy.93, pred[]{:T(512)S(6)} %eq.32), kind=kLoop, calls=%fused_computation.23 | loop fusion | flops 2359296 | bytes 1048577 | tf_op jit(solution)/shard_map/jit(_where)/select_n | solution.py:408
  88.1 18.1 %gather_rows.1 = (bf16[256,2048]{1,0:T(8,128)(2,1)}, bf16[256,128]{1,0:T(8,128)(2,1)}, bf16[256,128]{1,0:T(8,128)(2,1)}) custom-call(bf16[16,1152]{1,0:T(8,128)(2,1)} %concatenate.40.a_ref, bf16[16,1024]{1,0:T(8,128)(2,1)} %get-tuple-element.11.b_ref, bf16[2048,128]{1,0:T(8,128)(2,1)} %maximum_select_fusion.2.gate_ref, ...), custom_call_target="tpu_custom_call" | custom-call | tf_op jit(solution)/shard_map/gather_rows/pallas_call | solution.py:273
  108.3 3.0 %fusion.25 = f32[256,2048]{1,0:T(8,128)} fusion(bf16[256,2048]{1,0:T(8,128)(2,1)} %get-tuple-element.7, s32[256]{0:T(256)S(1)} %broadcast_select_fusion.1), kind=kOutput, calls=%fused_computation.34 | convolution fusion | flops 268500992 | bytes 3146752 | tf_op jit(solution)/shard_map/dot_general | solution.py:454
  112.1 2.2 %fusion = bf16[256,2048]{1,0:T(8,128)(2,1)S(1)} fusion(f32[256,2048]{1,0:T(8,128)} %fusion.25, bf16[256,2048]{1,0:T(8,128)(2,1)S(1)} %collective-permute-done.5, s32[256]{0:T(256)S(1)} %broadcast_select_fusion), kind=kOutput, calls=%fused_computation.2 | convolution fusion | flops 269549568 | bytes 4195328 | tf_op jit(solution)/shard_map/dot_general | solution.py:455
  116.0 4.2 %fusion.1 = bf16[32,8,2048]{2,1,0:T(8,128)(2,1)} fusion(bf16[1,512,2048]{2,1,0:T(8,128)(2,1)S(1)} %copy-done, bf16[256,2048]{1,0:T(8,128)(2,1)} %copy-done.2, bf16[1,2048,512]{2,1,0:T(8,128)(2,1)} %param.39, f32[256,512]{1,0:T(8,128)S(1)} %fusion.5), kind=kOutput, calls=%fused_computation.3 | convolution fusion | flops 1075052544 | bytes 6815744 | tf_op jit(solution)/shard_map/dot_general | solution.py:462
  120.3 3.8 %all-to-all-start = ((bf16[32,8,2048]{2,1,0:T(8,128)(2,1)}), bf16[32,8,2048]{2,1,0:T(8,128)(2,1)S(1)}, u32[]{:S(2)}, u32[]{:S(2)}) async-start(bf16[32,8,2048]{2,1,0:T(8,128)(2,1)} %fusion.1), calls=%async_computation | async-start | bytes 2097152 | tf_op jit(solution)/shard_map/all_to_all | solution.py:465
  126.4 1.8 %convolution_convert_fusion.4 = bf16[16,128]{1,0:T(8,128)(2,1)} fusion(bf16[16,2048]{1,0:T(8,128)(2,1)S(1)} %fusion.28, bf16[2048,128]{1,0:T(8,128)(2,1)} %param.29), kind=kOutput, calls=%fused_computation.19 | convolution fusion | flops 8390656 | bytes 593920 | tf_op jit(solution)/shard_map/dot_general | solution.py:420
  128.2 1.8 %convolution_convert_fusion.3 = bf16[16,128]{1,0:T(8,128)(2,1)} fusion(bf16[16,2048]{1,0:T(8,128)(2,1)S(1)} %fusion.28, bf16[2048,128]{1,0:T(8,128)(2,1)} %param.30), kind=kOutput, calls=%fused_computation.18 | convolution fusion | flops 8390656 | bytes 593920 | tf_op jit(solution)/shard_map/dot_general | solution.py:421
  130.2 1.4 fusion.40
  131.6 3.0 %maximum_select_fusion.4.w_ref = bf16[2048,128]{1,0:T(8,128)(2,1)} fusion(bf16[2048,64]{1,0:T(8,128)(2,1)} %collective-permute-done.6, bf16[2048,64]{1,0:T(8,128)(2,1)} %copy.100, pred[]{:T(512)S(6)} %eq.32), kind=kLoop, calls=%fused_computation.25 | loop fusion | flops 2359296 | bytes 1048577 | tf_op jit(solution)/shard_map/jit(_where)/select_n | solution.py:408
  134.6 35.4 %down_project.1 = bf16[16,2048]{1,0:T(8,128)(2,1)} custom-call(bf16[128,128]{1,0:T(8,128)(2,1)} %get-tuple-element.10.a_ref, bf16[128,128]{1,0:T(8,128)(2,1)} %get-tuple-element.9.b_ref, f32[1,2048]{1,0:T(1,128)} %bitcast.33, bf16[2048,128]{1,0:T(8,128)(2,1)} %maximum_select_fusion.4.w_ref), custom_call_target="tpu_custom_call" | custom-call | tf_op jit(solution)/shard_map/down_project/pallas_call | solution.py:293
  170.0 1.2 convolution_multiply_fusion
  171.2 1.2 reshape.108
  (90 shorter events, 16.9 us)
Async XLA Ops:
  0.6 115.4 %copy-start = (bf16[1,512,2048]{2,1,0:T(8,128)(2,1)S(1)}, bf16[1,512,2048]{2,1,0:T(8,128)(2,1)}, u32[]{:S(2)}) copy-start(bf16[1,512,2048]{2,1,0:T(8,128)(2,1)} %param.40) | copy-start | bytes 6291460
  0.6 5.8 %copy-start.4 = (bf16[2048,64]{0,1:T(8,128)(2,1)S(1)}, bf16[2048,64]{0,1:T(8,128)(2,1)}, u32[]{:S(2)}) copy-start(bf16[2048,64]{0,1:T(8,128)(2,1)} %param.28) | copy-start | bytes 786436
  0.7 6.8 %copy-start.1 = (bf16[16,2048]{1,0:T(8,128)(2,1)S(1)}, bf16[16,2048]{1,0:T(8,128)(2,1)}, u32[]{:S(2)}) copy-start(bf16[16,2048]{1,0:T(8,128)(2,1)} %param.23) | copy-start | bytes 196612
  0.7 6.9 %copy-start.14 = (s32[16]{0:T(128)S(1)}, s32[16]{0:T(128)}, u32[]{:S(2)}) copy-start(s32[16]{0:T(128)} %param.34) | copy-start | bytes 196
  0.7 7.0 %copy-start.10 = (s32[16,6]{0,1:T(8,128)S(1)}, s32[16,6]{0,1:T(8,128)}, u32[]{:S(2)}) copy-start(s32[16,6]{0,1:T(8,128)} %param.35) | copy-start | bytes 1156
  0.7 7.0 %copy-start.7 = (f32[2048]{0:T(1024)S(1)}, f32[2048]{0:T(1024)}, u32[]{:S(2)}) copy-start(f32[2048]{0:T(1024)} %param.27) | copy-start | bytes 24580
  2.1 80.8 %collective-permute-start.3 = (bf16[2048,64]{1,0:T(8,128)(2,1)S(1)}, bf16[2048,64]{1,0:T(8,128)(2,1)}, u32[]{:S(2)}, u32[]{:S(2)}) collective-permute-start(bf16[2048,64]{1,0:T(8,128)(2,1)S(1)} %copy.96), channel_id=1, source_target_pairs={{0,1},{1,0},{2,3},{3,2},{4,5},{5,4},{6,7},{7,6},{8,9},{9,8},{10,11... | collective-permute-start | bytes 786440 | tf_op jit(solution)/shard_map/ppermute | solution.py:407
  3.9 39.0 %copy-start.12 = (f32[32]{0:T(128)S(1)}, f32[32]{0:T(128)}, u32[]{:S(2)}) copy-start(f32[32]{0:T(128)} %param.31) | copy-start | bytes 388
  3.9 81.6 %collective-permute-start.2 = (bf16[2048,64]{1,0:T(8,128)(2,1)S(1)}, bf16[2048,64]{1,0:T(8,128)(2,1)}, u32[]{:S(2)}, u32[]{:S(2)}) collective-permute-start(bf16[2048,64]{1,0:T(8,128)(2,1)S(1)} %copy.93), channel_id=1, source_target_pairs={{0,1},{1,0},{2,3},{3,2},{4,5},{5,4},{6,7},{7,6},{8,9},{9,8},{10,11... | collective-permute-start | bytes 786440 | tf_op jit(solution)/shard_map/ppermute | solution.py:407
  5.9 49.2 %collective-permute-start.1 = (bf16[2048,64]{1,0:T(8,128)(2,1)}, bf16[2048,64]{1,0:T(8,128)(2,1)}, u32[]{:S(2)}, u32[]{:S(2)}) collective-permute-start(bf16[2048,64]{1,0:T(8,128)(2,1)} %copy.87), channel_id=1, source_target_pairs={{0,1},{1,0},{2,3},{3,2},{4,5},{5,4},{6,7},{7,6},{8,9},{9,8},{10,11... | collective-permute-start | bytes 786440 | tf_op jit(solution)/shard_map/ppermute | solution.py:407
  7.4 2.3 %collective-permute-start = (bf16[2048,64]{1,0:T(8,128)(2,1)}, bf16[2048,64]{1,0:T(8,128)(2,1)}, u32[]{:S(2)}, u32[]{:S(2)}) collective-permute-start(bf16[2048,64]{1,0:T(8,128)(2,1)} %copy.84), channel_id=1, source_target_pairs={{0,1},{1,0},{2,3},{3,2},{4,5},{5,4},{6,7},{7,6},{8,9},{9,8},{10,11... | collective-permute-start | bytes 786440 | tf_op jit(solution)/shard_map/ppermute | solution.py:407
  53.4 27.2 %copy-start.8 = (f32[2048]{0:T(1024)S(1)}, f32[2048]{0:T(1024)}, u32[]{:S(2)}) copy-start(f32[2048]{0:T(1024)} %param.33) | copy-start | bytes 24580
  106.1 5.2 %collective-permute-start.4 = (bf16[256,128]{1,0:T(8,128)(2,1)}, bf16[256,128]{1,0:T(8,128)(2,1)S(1)}, u32[]{:S(2)}, u32[]{:S(2)}) collective-permute-start(bf16[256,128]{1,0:T(8,128)(2,1)} %get-tuple-element.6), channel_id=1, source_target_pairs={{0,1},{1,0},{2,3},{3,2},{4,5},{5,4},{6,7},{7,6},{8,9},{9,8},{10,11... | collective-permute-start | bytes 196616 | tf_op jit(solution)/shard_map/ppermute | solution.py:439
  107.8 4.3 %collective-permute-start.5 = (bf16[256,2048]{1,0:T(8,128)(2,1)}, bf16[256,2048]{1,0:T(8,128)(2,1)S(1)}, u32[]{:S(2)}, u32[]{:S(2)}) collective-permute-start(bf16[256,2048]{1,0:T(8,128)(2,1)} %get-tuple-element.7), channel_id=1, source_target_pairs={{0,1},{1,0},{2,3},{3,2},{4,5},{5,4},{6,7},{7,6},{8,9},{9,8},{10,11... | collective-permute-start | bytes 3145736 | tf_op jit(solution)/shard_map/ppermute | solution.py:438
  112.1 3.2 %copy-start.13 = (bf16[1,2048,512]{2,1,0:T(8,128)(2,1)S(1)}, bf16[1,2048,512]{2,1,0:T(8,128)(2,1)}, u32[]{:S(2)}) copy-start(bf16[1,2048,512]{2,1,0:T(8,128)(2,1)} %param.38) | copy-start | bytes 6291460
  114.3 1.0 copy-start.2
  120.2 3.8 %copy-start.5 = (bf16[2048,64]{0,1:T(8,128)(2,1)S(1)}, bf16[2048,64]{0,1:T(8,128)(2,1)}, u32[]{:S(2)}) copy-start(bf16[2048,64]{0,1:T(8,128)(2,1)} %param.44) | copy-start | bytes 786436
  120.2 5.5 %copy-start.11 = (f32[16,6]{0,1:T(8,128)S(1)}, f32[16,6]{0,1:T(8,128)}, u32[]{:S(2)}) copy-start(f32[16,6]{0,1:T(8,128)} %param.37) | copy-start | bytes 1156
  120.2 6.1 %copy-start.9 = (f32[2048]{0:T(1024)S(1)}, f32[2048]{0:T(1024)}, u32[]{:S(2)}) copy-start(f32[2048]{0:T(1024)} %param.45) | copy-start | bytes 24580
  120.3 49.7 %all-to-all-start = ((bf16[32,8,2048]{2,1,0:T(8,128)(2,1)}), bf16[32,8,2048]{2,1,0:T(8,128)(2,1)S(1)}, u32[]{:S(2)}, u32[]{:S(2)}) async-start(bf16[32,8,2048]{2,1,0:T(8,128)(2,1)} %fusion.1), calls=%async_computation | async-start | bytes 2097152 | tf_op jit(solution)/shard_map/all_to_all | solution.py:465
  125.1 6.5 %collective-permute-start.6 = (bf16[2048,64]{1,0:T(8,128)(2,1)}, bf16[2048,64]{1,0:T(8,128)(2,1)}, u32[]{:S(2)}, u32[]{:S(2)}) collective-permute-start(bf16[2048,64]{1,0:T(8,128)(2,1)} %copy.100), channel_id=1, source_target_pairs={{0,1},{1,0},{2,3},{3,2},{4,5},{5,4},{6,7},{7,6},{8,9},{9,8},{10,11... | collective-permute-start | bytes 786440 | tf_op jit(solution)/shard_map/ppermute | solution.py:407
  170.0 2.8 %copy-start.3 = (bf16[16,2048]{1,0:T(8,128)(2,1)S(1)}, bf16[16,2048]{1,0:T(8,128)(2,1)}, u32[]{:S(2)}) copy-start(bf16[16,2048]{1,0:T(8,128)(2,1)} %project.3) | copy-start | bytes 196612
  170.0 2.8 %copy-start.6 = (bf16[16,2048]{1,0:T(8,128)(2,1)S(1)}, bf16[16,2048]{1,0:T(8,128)(2,1)}, u32[]{:S(2)}) copy-start(bf16[16,2048]{1,0:T(8,128)(2,1)} %down_project.1) | copy-start | bytes 196612
where the time goes:
time: 174 us; the launch traced here: 173 us
  Pallas kernels  113 us (65%)
  other arithmetic  19.5 us (11%)
  local copies, waits for them, and re-layouts  17.3 us (10%)
  matrix products  15.3 us (9%)
  starting transfers between devices  5.86 us (3%)
    pallas_call x2, Pallas kernels, project(): pl.pallas_call(functools.partial(project_kernel, chips), out_shape=jax.Sh...  50.1 us
    pallas_call x1, Pallas kernels, down_project(): pl.pallas_call(functools.partial(down_kernel, chips), out_shape=jax.Shape...  35.4 us
    pallas_call x1, Pallas kernels, gather_rows(): pl.pallas_call(functools.partial(gather_kernel, chips), out_shape=(jax.Sh...  18.1 us
    select_n x5, other arithmetic, both(): jnp.where(first, jnp.concatenate([own, other], axis=-1), jnp.concatenate(...  14 us
    pallas_call x1, Pallas kernels, stick_read(): pl.pallas_call(stick_kernel, out_shape=jax.ShapeDtypeStruct((batch, HEADS...  9.84 us
    unnamed x35, local copies, waits for them, and re-layouts  7.7 us
    dot_general x1, matrix products, shards(): jnp.dot(expert_hidden, expert_down_w[0], preferred_element_type=jnp.float32)  4.23 us
    all_to_all x1, starting transfers between devices, shards(): lax.all_to_all(served.reshape(devices, capacity, width), 'ep', split_axis...  3.83 us
  transfers between devices with their start and end apart: 8, of which 1 were waited for; matrix products, arithmetic and copies ran while one was open for 21% of the time, Pallas kernels for 55%

commit v1 on v0

--- a/solution.py
+++ b/solution.py
@@ -1,4 +1,5 @@
 import functools
+import types
 
 import jax
 import jax.numpy as jnp
@@ -489,6 +490,698 @@
     return (mixed_out.astype(jnp.bfloat16), new_keys, new_values)
 
 
+LOG2E = 1.4426950408889634
+DEAD = -1e30
+TRANSPOSED = (((1,), (1,)), ((), ()))
+
+
+def dot_t(a, b):
+    return lax.dot_general(a, b, TRANSPOSED, preferred_element_type=jnp.float32)
+
+
+def dot(a, b):
+    return jnp.dot(a, b, preferred_element_type=jnp.float32)
+
+
+def remote(src, dst, send, recv, device):
+    return pltpu.make_async_remote_copy(
+        src_ref=src, dst_ref=dst, send_sem=send, recv_sem=recv, device_id=device, device_id_type=MESH
+    )
+
+
+class Grid(Place):
+    def __init__(self, chips):
+        super().__init__(chips)
+        self.partner = (self.chip * 2 + 1 - self.core,)
+        self.depth = self.dims[0]
+        self.plane = chips // self.depth
+
+    def on(self, z, dy=0, dx=0):
+        depth, height, width = self.dims
+        y = lax.rem(self.y + dy, height)
+        x = lax.rem(self.x + dx, width)
+        return (z * height + y) * width + x
+
+    def turn(self, axis):
+        return (1, 0) if axis == "y" else (0, 1)
+
+    def sweep(self, step):
+        toward = 1 - 2 * (self.z // (self.depth // 2))
+        return lax.rem(self.z + step * toward + self.depth, self.depth)
+
+    def enter(self):
+        barrier = pltpu.get_barrier_semaphore()
+        for step in range(1, self.chips):
+            other = lax.rem(self.chip + step, self.chips)
+            pl.semaphore_signal(barrier, inc=1, device_id=self.device(other), device_id_type=MESH)
+        pl.semaphore_signal(barrier, inc=1, device_id=self.partner, device_id_type=MESH)
+        pl.semaphore_wait(barrier, self.chips)
+
+
+class Gather:
+    def __init__(self, place, pieces):
+        self.place = place
+        self.pieces = pieces
+
+    def copy(self, piece, kind, origin, target):
+        view, send, recv, _ = self.pieces[piece]
+        z = origin // self.place.plane
+        return remote(view(origin), view(origin), send.at[kind * self.place.depth + z], recv.at[origin],
+                      self.place.device(target))
+
+    def arrive(self, piece, origin):
+        self.copy(piece, 0, origin, self.place.chip).wait_recv()
+
+    def turns(self, piece):
+        first, second = self.pieces[piece][3]
+        return self.place.turn(first), self.place.turn(second)
+
+    def across(self, piece, z):
+        place = self.place
+        first, second = self.turns(piece)
+        self.copy(piece, 2, place.on(z), place.on(place.z, *first)).start()
+        self.copy(piece, 3, place.on(z), place.on(place.z, *second)).start()
+
+    def corner(self, piece, z):
+        place = self.place
+        first, second = self.turns(piece)
+        origin = place.on(z, *first)
+        self.arrive(piece, origin)
+        self.copy(piece, 4, origin, place.on(place.z, *second)).start()
+
+    def start(self):
+        place, z, depth = self.place, self.place.z, self.place.depth
+        every = range(len(self.pieces))
+
+        @pl.when(z < depth - 1)
+        def _():
+            for piece in every:
+                self.copy(piece, 0, place.chip, place.on(z + 1)).start()
+
+        @pl.when(z > 0)
+        def _():
+            for piece in every:
+                self.copy(piece, 1, place.chip, place.on(z - 1)).start()
+
+        for piece in every:
+            self.across(piece, z)
+
+    def relay(self):
+        place, z, depth = self.place, self.place.z, self.place.depth
+        every = range(len(self.pieces))
+        for piece in every:
+            self.corner(piece, z)
+        for step in range(1, depth):
+
+            @pl.when(z >= step)
+            def _():
+                for piece in every:
+                    self.arrive(piece, place.on(z - step))
+
+                    @pl.when(z < depth - 1)
+                    def _():
+                        self.copy(piece, 0, place.on(z - step), place.on(z + 1)).start()
+
+                    self.across(piece, z - step)
+
+            @pl.when(z + step < depth)
+            def _():
+                for piece in every:
+                    self.arrive(piece, place.on(z + step))
+
+                    @pl.when(z > 0)
+                    def _():
+                        self.copy(piece, 1, place.on(z + step), place.on(z - 1)).start()
+
+                    self.across(piece, z + step)
+
+            @pl.when(z >= step)
+            def _():
+                for piece in every:
+                    self.corner(piece, z - step)
+
+            @pl.when(z + step < depth)
+            def _():
+                for piece in every:
+                    self.corner(piece, z + step)
+
+    def rest(self, piece, z):
+        first, second = self.turns(piece)
+        self.arrive(piece, self.place.on(z, *second))
+        self.arrive(piece, self.place.on(z, 1, 1))
+
+    def finish(self):
+        place, depth = self.place, self.place.depth
+        for piece in range(len(self.pieces)):
+            for z in range(depth):
+                for kind in (2, 3, 4):
+                    self.copy(piece, kind, place.on(z), place.chip).wait_send()
+
+                @pl.when((place.z >= z) & (place.z < depth - 1))
+                def _():
+                    self.copy(piece, 0, place.on(z), place.chip).wait_send()
+
+                @pl.when((place.z <= z) & (place.z > 0))
+                def _():
+                    self.copy(piece, 1, place.on(z), place.chip).wait_send()
+
+
+def norm_rows(values, gain):
+    square = jnp.mean(values * values, axis=-1, keepdims=True)
+    return (values * lax.rsqrt(square + epsilon) * gain).astype(jnp.bfloat16)
+
+
+ORDERS = (("x", "y"), ("y", "x"))
+
+
+def layer_kernel(
+    chips, names,
+    lens_ref, bias_ref, tokens_ref, gain1_ref, gain2_ref, hgain_ref, logit_ref,
+    member_ref, mweight_ref, group_ref, ggate_ref,
+    keys_hbm, values_hbm, wq_hbm, wo_hbm, wg_hbm, wu_hbm, wd_hbm, wk_hbm, wv_hbm, eg_hbm, eu_hbm, ed_hbm,
+    out_ref, newk_ref, newv_ref,
+    *scratch,
+):
+    s = types.SimpleNamespace(**dict(zip(names, scratch)))
+    place = Grid(chips)
+    me = place.chip * 2 + place.core
+    chip, z, depth, plane = place.chip, place.z, place.depth, place.plane
+    seq, width = tokens_ref.shape
+    half = width // 2
+    rows = chips * seq
+    lanes = LANES
+    experts = chips * 2
+    part = plane * seq
+    bf16 = jnp.bfloat16
+
+    own_rows = pl.ds(pl.multiple_of(place.core * 64, 64), 64)
+    weights = ((s.wq, wq_hbm), (s.wo, wo_hbm), (s.wg, wg_hbm), (s.wu, wu_hbm))
+    local = types.SimpleNamespace()
+
+    def fetch(src, dst, index):
+        copy = pltpu.make_async_copy(src, dst, s.local_sem.at[index])
+        copy.start()
+        return copy
+
+    local.wq, local.wo, local.wg, local.wu = (
+        fetch(src, dst.at[own_rows], i) for i, (dst, src) in enumerate(weights)
+    )
+    local.wk = fetch(wk_hbm, s.wk, 4)
+    local.wv = fetch(wv_hbm, s.wv, 5)
+    local.keys = fetch(keys_hbm, s.keys, 6)
+    local.values = fetch(values_hbm, s.values, 7)
+    local.eg = fetch(eg_hbm.at[0], s.eg, 8)
+    local.eu = fetch(eu_hbm.at[0], s.eu, 9)
+    local.ed = fetch(ed_hbm.at[0], s.ed, 10)
+
+    place_of = lax.broadcasted_iota(jnp.int32, (lanes, seq), 0)
+    expert = lax.rem(place_of, experts)
+    combine = jnp.zeros((lanes, seq), jnp.float32)
+    for k in range(TOP_K):
+        named = group_ref[...] * PER_GROUP + member_ref[k : k + 1, :]
+        weight = ggate_ref[...] * mweight_ref[k : k + 1, :]
+        combine = jnp.where(expert == named, weight, combine)
+    high = combine.astype(bf16).astype(jnp.float32)
+    notes = jnp.where(place_of < experts, high, jnp.where(place_of < 2 * experts, combine - high, 0.0))
+    diagonal = lax.broadcasted_iota(jnp.int32, (seq, seq), 0) == lax.broadcasted_iota(jnp.int32, (seq, seq), 1)
+    notes = dot_t(jnp.where(diagonal, 1.0, 0.0).astype(bf16), notes.astype(bf16))
+    slots1, slots2, slots3 = s.slots1, s.slots2, s.slots3
+    slots1[chip, :, :lanes] = notes.astype(bf16)
+    slots1[chip, :, lanes:] = tokens_ref[...]
+
+    place.enter()
+
+    cut = lanes + half
+    gather1 = Gather(place, (
+        (lambda o: slots1.at[o, :, pl.ds(0, cut)], s.send1a, s.recv1a, ORDERS[0]),
+        (lambda o: slots1.at[o, :, pl.ds(cut, half)], s.send1b, s.recv1b, ORDERS[1]),
+    ))
+    gather1.start()
+    swaps = [
+        remote(src, dst.at[own_rows], s.swap_send.at[i], s.swap_recv.at[i], place.partner)
+        for i, (dst, src) in enumerate(weights)
+    ]
+    for swap in swaps:
+        swap.start()
+    gather1.relay()
+    local.wq.wait()
+    swaps[0].wait_recv()
+
+    tiles, landed = s.tiles, s.landed
+
+    def tile_copy(index, target):
+        return remote(tiles.at[target], landed.at[chip], s.tile_send.at[index], s.tile_recv.at[chip],
+                      place.device(target))
+
+    for step in range(depth):
+        zo = place.sweep(step)
+        for piece in range(2):
+            gather1.rest(piece, zo)
+        at = pl.ds(zo * plane, plane)
+        rows_f = slots1[at, :, lanes:].reshape(part, width).astype(jnp.float32)
+        product = dot_t(norm_rows(rows_f, gain1_ref[...]), s.wq[...])
+        tiles[at] = product.astype(bf16).reshape(plane, seq, lanes)
+        for dy in (1, 0):
+            for dx in (1, 0):
+                target = place.on(zo, dy, dx)
+                if (step, dy, dx) == (0, 0, 0):
+                    landed[chip] = tiles[chip]
+                else:
+                    tile_copy(step * plane + dy * 2 + dx, target).start()
+
+    own_normed = norm_rows(tokens_ref[...].astype(jnp.float32), gain1_ref[...])
+    local.wk.wait()
+    local.wv.wait()
+    newk_ref[...] = dot(own_normed, s.wk[...]).astype(bf16)
+    newv_ref[...] = dot(own_normed, s.wv[...]).astype(bf16)
+
+    for step in range(1, chips):
+        origin = lax.rem(chip + step, chips)
+        remote(tiles.at[origin], landed.at[origin], s.tile_send.at[0], s.tile_recv.at[origin],
+               place.device(chip)).wait_recv()
+
+    def down_copy(target):
+        columns = pl.ds(pl.multiple_of(target * lanes, lanes), lanes)
+        return remote(wd_hbm.at[:, columns], s.wd.at[chip, place.core], s.down_send.at[target],
+                      s.down_recv.at[chip], place.device(target))
+
+    for step in range(1, chips):
+        down_copy(lax.rem(chip + step, chips)).start()
+    local.wd = fetch(wd_hbm.at[:, pl.ds(pl.multiple_of(chip * lanes, lanes), lanes)], s.wd.at[chip, place.core], 11)
+
+    heads, mixed = s.heads, s.mixed
+    for j in range(chips):
+        heads[:, j, :] = landed[j].astype(jnp.float32)
+    local.keys.wait()
+    local.values.wait()
+    span = s.keys.shape[1]
+    blocks = span // LANES
+    row = lax.broadcasted_iota(jnp.int32, (2 * LANES, 2 * LANES), 0)
+    column = lax.broadcasted_iota(jnp.int32, (2 * LANES, 2 * LANES), 1)
+    after = ((lax.rem(row, LANES) > column) | (column >= LANES)).astype(bf16)
+    position = lax.broadcasted_iota(jnp.int32, (HEADS, span), 1)
+    jrow = lax.broadcasted_iota(jnp.int32, (chips, LANES), 0)
+    jlane = lax.broadcasted_iota(jnp.int32, (chips, LANES), 1)
+    early = jrow < chips // KV_HEADS
+    own = (jlane // HEAD_DIM) == (jrow // (chips // KV_HEADS))
+    head_row = lax.broadcasted_iota(jnp.int32, (HEADS, LANES), 0)
+    bias = jnp.zeros((HEADS, LANES), jnp.float32)
+    for head in range(HEADS):
+        bias = jnp.where(head_row == (head % 2) * chips + head // 2, bias_ref[head] * LOG2E, bias)
+    bias = jnp.concatenate([bias] * blocks, axis=1)
+
+    def attend(item):
+        even = heads[item]
+        turned = pltpu.roll(even, HEAD_DIM, axis=1)
+        query = jnp.concatenate([
+            jnp.where(own, jnp.where(early, even, turned), 0.0),
+            jnp.where(own, jnp.where(early, turned, even), 0.0),
+        ], axis=0).astype(bf16)
+        scores = dot_t(query, s.keys[item]) * (HEAD_DIM ** (-0.5) * LOG2E) + bias
+        scores = jnp.where(position < lens_ref[item], scores, DEAD)
+        soft = jnp.maximum(scores, 0.0) + jnp.log(1.0 + jnp.exp2(-jnp.abs(scores))) * LOG2E
+        stacked = jnp.concatenate([soft[:, n * LANES : (n + 1) * LANES] for n in range(blocks)], axis=0)
+        top = stacked.astype(bf16)
+        low = (stacked - top.astype(jnp.float32)).astype(bf16)
+        sums = dot(jnp.concatenate([top, low], axis=1), after)
+        sums = sums
+        carried = jnp.zeros((HEADS, LANES), jnp.float32)
+        pieces = [None] * blocks
+        for n in range(blocks - 1, -1, -1):
+            band = sums[n * HEADS : (n + 1) * HEADS]
+            spent = stacked[n * HEADS : (n + 1) * HEADS] + band[:, :LANES] + carried
+            pieces[n] = jnp.exp2(scores[:, n * LANES : (n + 1) * LANES] - spent).astype(bf16)
+            carried = carried + band[:, LANES:]
+        found = dot(jnp.concatenate(pieces, axis=1), s.values[item])
+        first, second = found[:chips], found[chips:]
+        mixed[item] = jnp.where(
+            jlane < HEAD_DIM,
+            jnp.where(early, first, pltpu.roll(first, HEAD_DIM, axis=1)),
+            jnp.where(early, pltpu.roll(second, HEAD_DIM, axis=1), second),
+        )
+
+    together = 4 if seq % 4 == 0 else 1
+
+    @pl.loop(0, seq // together)
+    def _(index):
+        for t in range(together):
+            attend(index * together + t)
+
+    for j in range(chips):
+        slots2[chip, :, j * LANES : (j + 1) * LANES] = mixed[:, j, :].astype(bf16)
+
+    gather2 = Gather(place, (
+        (lambda o: slots2.at[o, :, pl.ds(0, half)], s.send2a, s.recv2a, ORDERS[0]),
+        (lambda o: slots2.at[o, :, pl.ds(half, half)], s.send2b, s.recv2b, ORDERS[1]),
+    ))
+    gather2.start()
+    gather2.relay()
+    local.wo.wait()
+    swaps[1].wait_recv()
+    for step in range(depth):
+        zo = place.sweep(step)
+        for piece in range(2):
+            gather2.rest(piece, zo)
+        product = dot_t(slots2[pl.ds(zo * plane, plane)].reshape(part, width), s.wo[...])
+        slots3[chip, pl.ds(pl.multiple_of(zo * part, part), part), :] = product.astype(bf16)
+
+    gather3 = Gather(place, (
+        (lambda o: slots3.at[o, pl.ds(0, rows // 2), :], s.send3a, s.recv3a, ORDERS[0]),
+        (lambda o: slots3.at[o, pl.ds(rows // 2, rows // 2), :], s.send3b, s.recv3b, ORDERS[1]),
+    ))
+    gather3.start()
+    gather3.relay()
+    local.wd.wait()
+    for step in range(1, chips):
+        origin = lax.rem(chip + step, chips)
+        remote(s.wd.at[origin, place.core], s.wd.at[origin, place.core], s.down_send.at[0],
+               s.down_recv.at[origin], place.device(chip)).wait_recv()
+    down_swap = remote(s.wd.at[:, place.core], s.wd.at[:, place.core], s.swap_send.at[4],
+                       s.swap_recv.at[4], place.partner)
+    down_swap.start()
+    for step in range(depth):
+        for piece in range(2):
+            gather3.rest(piece, place.sweep(step))
+
+    rows_own, rows_other = s.rows_own, s.rows_other
+    row_copies = []
+    for block in range(depth):
+        at = slice(block * part, (block + 1) * part)
+        token = slots1[block * plane : (block + 1) * plane, :, lanes:].reshape(part, width).astype(jnp.float32)
+        projected = jnp.concatenate([slots3[c, at, :] for c in range(chips)], axis=1).astype(jnp.float32)
+        rows_own[at, :width] = norm_rows(token + projected, gain2_ref[...])
+        rows_own[at, width:] = slots1[block * plane : (block + 1) * plane, :, :lanes].reshape(part, lanes)
+        row_copies.append(remote(rows_own.at[at], rows_other.at[at], s.row_send.at[block],
+                                 s.row_recv.at[block], place.partner))
+        row_copies[-1].start()
+
+    local.wg.wait()
+    local.wu.wait()
+    swaps[2].wait_recv()
+    swaps[3].wait_recv()
+    normed = rows_own[:, :width]
+    gate = dot_t(normed, s.wg[...])
+    hidden = jax.nn.silu(gate) * dot_t(normed, s.wu[...])
+    s.hidden[...] = hidden
+    squares = jnp.broadcast_to(jnp.sum(hidden * hidden, axis=1, keepdims=True), (rows, LANES))
+    s.squares[chip] = jnp.transpose(squares)[:1]
+
+    def square_copy(target):
+        return remote(s.squares.at[chip], s.squares.at[chip], s.square_send.at[target],
+                      s.square_recv.at[chip], place.device(target))
+
+    for step in range(1, chips):
+        square_copy(lax.rem(chip + step, chips)).start()
+
+    local.eg.wait()
+    local.eu.wait()
+
+    def expert_hidden(ref):
+        gate_pre = dot(ref[:, :width], s.eg[...])
+        return (jax.nn.silu(gate_pre) * dot(ref[:, :width], s.eu[...])).astype(bf16)
+
+    note_lane = lax.broadcasted_iota(jnp.int32, (rows, LANES), 1)
+    mine = (note_lane == me) | (note_lane == me + experts)
+
+    def weight_of(ref):
+        return jnp.sum(jnp.where(mine, ref[:, width:].astype(jnp.float32), 0.0), axis=1, keepdims=True)
+
+    s.hid_own[...] = expert_hidden(rows_own)
+    for copy in row_copies:
+        copy.wait_recv()
+    s.hid_other[...] = expert_hidden(rows_other)
+    local.ed.wait()
+    chunk = width // 4
+    weight_other = weight_of(rows_other)
+    gift_copies = []
+    for c in range(4):
+        at = slice(c * chunk, (c + 1) * chunk)
+        served = dot(s.hid_other[...], s.ed[:, at])
+        s.gift[c] = jnp.where(weight_other != 0.0, served * weight_other, 0.0).astype(bf16)
+        gift_copies.append(remote(s.gift.at[c], s.given.at[c], s.gift_send.at[c],
+                                  s.gift_recv.at[c], place.partner))
+        gift_copies[-1].start()
+
+    for step in range(1, chips):
+        origin = lax.rem(chip + step, chips)
+        remote(s.squares.at[origin], s.squares.at[origin], s.square_send.at[0],
+               s.square_recv.at[origin], place.device(chip)).wait_recv()
+    total = s.squares[0]
+    for c in range(1, chips):
+        total = total + s.squares[c]
+    scale = lax.rsqrt(total / width + epsilon)
+    scale = jnp.transpose(jnp.broadcast_to(scale, (LANES, rows)))
+    gain = hgain_ref[:, pl.ds(pl.multiple_of(chip * lanes, lanes), lanes)]
+    dense = (s.hidden[...] * scale * gain).astype(bf16)
+    down_swap.wait_recv()
+    weight_own = weight_of(rows_own)
+    acc = s.acc
+
+    def first_index(zo, beside):
+        return zo * 2 + beside
+
+    def columns_of(piece):
+        return slice(piece * half, (piece + 1) * half)
+
+    def staged(piece, value, slot, dst, index, recv, target):
+        stage = s.stage
+        stage[piece, slot] = value.astype(bf16)
+        remote(stage.at[piece, slot], dst, s.sum_send.at[piece, index], recv, place.device(target)).start()
+
+    def first_dst(piece, zo, beside):
+        return s.sum1.at[piece, first_index(zo, beside)], s.sum1_recv.at[piece, first_index(zo, beside)]
+
+    def send_first(piece, step, beside):
+        first, second = (place.turn(a) for a in ORDERS[piece])
+        zo = place.sweep(step)
+        turn = (1, 1) if beside else first
+        dst, recv = first_dst(piece, zo, beside)
+        slot = step * 2 + beside
+        staged(piece, acc[place.on(zo, *turn), :, columns_of(piece)], slot, dst, slot, recv, place.on(z, *first))
+
+    def wait_into(ref, recv):
+        remote(ref, ref, s.sum_send.at[0, 0], recv, place.device(chip)).wait_recv()
+        return ref[...].astype(jnp.float32)
+
+    for piece in range(2):
+        for c in (2 * piece, 2 * piece + 1):
+            at = slice(c * chunk, (c + 1) * chunk)
+            served = dot(s.hid_own[...], s.ed[:, at])
+            value = jnp.where(weight_own != 0.0, served * weight_own, 0.0)
+            down = s.wd[c * (chips // 4) : (c + 1) * (chips // 4)].reshape(chunk, LANES)
+            value = value + jax.nn.sigmoid(logit_ref[:, at]) * dot_t(dense, down)
+            gift_copies[c].wait_recv()
+            value = value + s.given[c].astype(jnp.float32)
+            acc[:, :, at] = value.reshape(chips, seq, chunk)
+        for beside in (1, 0):
+            for step in range(depth - 1, -1, -1):
+                send_first(piece, step, beside)
+
+    base = 2 * depth
+    for step in range(depth - 1, -1, -1):
+        for piece in range(2):
+            first, second = (place.turn(a) for a in ORDERS[piece])
+            zo = place.sweep(step)
+            value = acc[place.on(zo, *second), :, columns_of(piece)] + wait_into(*first_dst(piece, zo, 1))
+            staged(piece, value, base + step, s.sum2.at[piece, zo], base + step,
+                   s.sum2_recv.at[piece, zo], place.on(z, *second))
+
+    def folded(piece, zo):
+        value = acc[place.on(zo), :, columns_of(piece)] + wait_into(*first_dst(piece, zo, 0))
+        return value + wait_into(s.sum2.at[piece, zo], s.sum2_recv.at[piece, zo])
+
+    base = 3 * depth
+
+    def along(piece, step, up):
+        zo = z + step if up else z - step
+        line, recv = (s.sum_up, s.sum_up_recv) if up else (s.sum_down, s.sum_down_recv)
+        acc[place.on(zo), :, columns_of(piece)] = folded(piece, zo)
+
+        @pl.when((z > 0) if up else (z < depth - 1))
+        def _():
+            acc[place.on(zo), :, columns_of(piece)] += wait_into(line.at[piece, zo], recv.at[piece, zo])
+
+        slot = base + zo
+        staged(piece, acc[place.on(zo), :, columns_of(piece)], slot, line.at[piece, zo], slot,
+               recv.at[piece, zo], place.on(z + 1 if up else z - 1))
+
+    for step in range(depth - 1, 0, -1):
+
+        @pl.when(z + step < depth)
+        def _():
+            for piece in range(2):
+                along(piece, step, True)
+
+        @pl.when(z >= step)
+        def _():
+            for piece in range(2):
+                along(piece, step, False)
+
+    own_at = pl.ds(pl.multiple_of(chip * seq, seq), seq)
+    for piece in range(2):
+        at = columns_of(piece)
+        value = tokens_ref[:, at].astype(jnp.float32)
+        value = value + jnp.concatenate(
+            [slots3[c, own_at, :] for c in range(piece * chips // 2, (piece + 1) * chips // 2)], axis=1
+        ).astype(jnp.float32)
+        acc[chip, :, at] = value + folded(piece, z)
+    for piece in range(2):
+
+        @pl.when(z > 0)
+        def _():
+            acc[chip, :, columns_of(piece)] += wait_into(s.sum_up.at[piece, z], s.sum_up_recv.at[piece, z])
+
+        @pl.when(z < depth - 1)
+        def _():
+            acc[chip, :, columns_of(piece)] += wait_into(s.sum_down.at[piece, z], s.sum_down_recv.at[piece, z])
+
+        out_ref[:, columns_of(piece)] = acc[chip, :, columns_of(piece)].astype(bf16)
+
+    for gather in (gather1, gather2, gather3):
+        gather.finish()
+    for step in range(1, chips):
+        tile_copy(step, lax.rem(chip + 1, chips)).wait_send()
+        target = lax.rem(chip + step, chips)
+        down_copy(target).wait_send()
+        square_copy(target).wait_send()
+    for copy in swaps + [down_swap] + row_copies + gift_copies:
+        copy.wait_send()
+
+    def sum_sent(piece, slot):
+        remote(s.stage.at[piece, slot], s.stage.at[piece, slot], s.sum_send.at[piece, slot],
+               s.sum1_recv.at[0, 0], place.device(chip)).wait_send()
+
+    for piece in range(2):
+        for slot in range(3 * depth):
+            sum_sent(piece, slot)
+        for zo in range(depth):
+
+            @pl.when(z != zo)
+            def _():
+                sum_sent(piece, 3 * depth + zo)
+
+
+def copy_kernel(a_ref, b_ref, c_ref, a_out, b_out, c_out):
+    a_out[...] = a_ref[...]
+    b_out[...] = b_ref[...]
+    c_out[...] = c_ref[...]
+
+
+def layer_scratch(chips, depth, seq, width, span, fe):
+    rows = chips * seq
+    bf16, f32, DMA = jnp.bfloat16, jnp.float32, pltpu.SemaphoreType.DMA
+    half = width // 2
+    return dict(
+        slots1=pltpu.VMEM((chips, seq, LANES + width), bf16),
+        slots2=pltpu.VMEM((chips, seq, width), bf16),
+        slots3=pltpu.VMEM((chips, rows, LANES), bf16),
+        keys=pltpu.VMEM((seq, span, LANES), bf16),
+        values=pltpu.VMEM((seq, span, LANES), bf16),
+        wk=pltpu.VMEM((width, LANES), bf16),
+        wv=pltpu.VMEM((width, LANES), bf16),
+        eg=pltpu.VMEM((width, fe), bf16),
+        eu=pltpu.VMEM((width, fe), bf16),
+        ed=pltpu.VMEM((fe, width), bf16),
+        wd=pltpu.VMEM((chips, 2, LANES // 2, LANES), bf16),
+        tiles=pltpu.VMEM((chips, seq, LANES), bf16),
+        landed=pltpu.VMEM((chips, seq, LANES), bf16),
+        heads=pltpu.VMEM((seq, chips, LANES), f32),
+        mixed=pltpu.VMEM((seq, chips, LANES), f32),
+        rows_own=pltpu.VMEM((rows, width + LANES), bf16),
+        rows_other=pltpu.VMEM((rows, width + LANES), bf16),
+        hidden=pltpu.VMEM((rows, LANES), f32),
+        squares=pltpu.VMEM((chips, 1, rows), f32),
+        hid_own=pltpu.VMEM((rows, fe), bf16),
+        hid_other=pltpu.VMEM((rows, fe), bf16),
+        gift=pltpu.VMEM((4, rows, width // 4), bf16),
+        given=pltpu.VMEM((4, rows, width // 4), bf16),
+        acc=pltpu.VMEM((chips, seq, width), f32),
+        stage=pltpu.VMEM((2, 4 * depth, seq, half), bf16),
+        sum1=pltpu.VMEM((2, 2 * depth, seq, half), bf16),
+        sum2=pltpu.VMEM((2, depth, seq, half), bf16),
+        sum_up=pltpu.VMEM((2, depth, seq, half), bf16),
+        sum_down=pltpu.VMEM((2, depth, seq, half), bf16),
+        local_sem=DMA((12,)),
+        swap_send=DMA((5,)),
+        swap_recv=DMA((5,)),
+        tile_send=DMA((chips,)),
+        tile_recv=DMA((chips,)),
+        down_send=DMA((chips,)),
+        down_recv=DMA((chips,)),
+        square_send=DMA((chips,)),
+        square_recv=DMA((chips,)),
+        row_send=DMA((depth,)),
+        row_recv=DMA((depth,)),
+        gift_send=DMA((4,)),
+        gift_recv=DMA((4,)),
+        sum_send=DMA((2, 4 * depth)),
+        sum1_recv=DMA((2, 2 * depth)),
+        sum2_recv=DMA((2, depth)),
+        sum_up_recv=DMA((2, depth)),
+        sum_down_recv=DMA((2, depth)),
+        wq=pltpu.VMEM((LANES, width), bf16),
+        wo=pltpu.VMEM((LANES, width), bf16),
+        wg=pltpu.VMEM((LANES, width), bf16),
+        wu=pltpu.VMEM((LANES, width), bf16),
+        send1a=DMA((5 * depth,)),
+        recv1a=DMA((chips,)),
+        send1b=DMA((5 * depth,)),
+        recv1b=DMA((chips,)),
+        send2a=DMA((5 * depth,)),
+        recv2a=DMA((chips,)),
+        send2b=DMA((5 * depth,)),
+        recv2b=DMA((chips,)),
+        send3a=DMA((5 * depth,)),
+        recv3a=DMA((chips,)),
+        send3b=DMA((5 * depth,)),
+        recv3b=DMA((chips,)),
+    )
+
+
+def fused_shards(
+    tokens, cache_keys, cache_values, cache_len, norm_gain_first, w_query, w_key, w_value, head_bias,
+    w_output, norm_gain_second, group_id, member, group_gate, member_weight, expert_gate_w,
+    expert_up_w, expert_down_w, dense_gate_w, dense_up_w, hidden_gain, dense_down_w, branch_logit,
+):
+    chips = lax.axis_size("ep") // 2
+    seq, width = tokens.shape
+    span = cache_keys.shape[1]
+    bf16 = jnp.bfloat16
+    scratch = layer_scratch(chips, torus_of(chips)[0], seq, width, span, expert_gate_w.shape[2])
+    smem = pl.BlockSpec(memory_space=pltpu.SMEM)
+    anywhere = pl.BlockSpec(memory_space=pl.ANY)
+    out_shape = (
+        jax.ShapeDtypeStruct((seq, width), bf16),
+        jax.ShapeDtypeStruct((seq, LANES), bf16),
+        jax.ShapeDtypeStruct((seq, LANES), bf16),
+    )
+    results = pl.pallas_call(
+        functools.partial(layer_kernel, chips, tuple(scratch)),
+        out_shape=out_shape,
+        in_specs=[smem] * 2 + [whole()] * 9 + [anywhere] * 12,
+        out_specs=(whole(),) * 3,
+        scratch_shapes=list(scratch.values()),
+        compiler_params=pltpu.CompilerParams(
+            collective_id=1, has_side_effects=True, vmem_limit_bytes=60 * 1024 * 1024
+        ),
+        name="layer",
+    )(
+        cache_len, head_bias, tokens, norm_gain_first[None], norm_gain_second[None], hidden_gain[None],
+        branch_logit[None], member.T, member_weight.T, group_id[None], group_gate[None],
+        cache_keys, cache_values, w_query.T, w_output.T, dense_gate_w.T, dense_up_w.T, dense_down_w.T,
+        w_key, w_value, expert_gate_w, expert_up_w, expert_down_w,
+    )
+    return pl.pallas_call(
+        copy_kernel, out_shape=out_shape, in_specs=[whole()] * 3, out_specs=(whole(),) * 3, name="results"
+    )(*results)
+
+
+def one_kernel(mesh):
+    chips = mesh.shape["ep"] // 2
+    depth, height, width = torus_of(chips)
+    return (height, width) == (2, 2) and chips * LANES == HEADS * HEAD_DIM and 4 * chips <= LANES
+
+
 def solution(mesh):
     in_specs = (
         P("ep", None),
@@ -516,4 +1209,5 @@
         P(),
     )
     out_specs = (P("ep", None), P("ep", None), P("ep", None))
-    return jax.shard_map(shards, mesh=mesh, in_specs=in_specs, out_specs=out_specs, check_vma=False)
+    body = fused_shards if one_kernel(mesh) else shards
+    return jax.shard_map(body, mesh=mesh, in_specs=in_specs, out_specs=out_specs, check_vma=False)

time: 174 us -> 107 us (0.61)
  other arithmetic: 19.5 us -> 0 us
  local copies, waits for them, and re-layouts: 17.3 us -> 0 us
  matrix products: 15.3 us -> 0 us
  Pallas kernels: 113 us -> 106 us
  starting transfers between devices: 5.86 us -> 0 us
    dot_general x10 -> x0, matrix products: 15.3 us -> none  [the longest x1 4.23 us: shards(): jnp.dot(expert_hidden, expert_down_w[0], preferred_element_type=jnp.float32)]
    select_n x7 -> x0, other arithmetic: 14.1 us -> none  [the longest x5 14 us: both(): jnp.where(first, jnp.concatenate([own, other], axis=-1), jnp.concatenate(...]
    unnamed x35 -> x0, local copies, waits for them, and re-layouts: 7.7 us -> none
    pallas_call x5 -> x2, Pallas kernels: 113 us -> 106 us  [the longest x1 104 us: fused_shards(): pl.pallas_call(functools.partial(layer_kernel, chips, tuple(scratch)), ou...]
    reshape x8 -> x0, local copies, waits for them, and re-layouts: 4.55 us -> none  [the longest x1 1.68 us: stick_read(): heads = queries.reshape(batch, HEADS, HEAD_DIM)]
    all_to_all x1 -> x0, starting transfers between devices: 3.83 us -> none  [shards(): lax.all_to_all(served.reshape(devices, capacity, width), 'ep', split_axis...]
    slice x4 -> x0, local copies, waits for them, and re-layouts: 3.26 us -> none  [the longest x1 1.41 us: down_project(): a, b = (hidden[:count // 2], hidden[count // 2:])]
    convert_element_type x5 -> x0, other arithmetic: 2.55 us -> none  [the longest x1 0.92 us: shards(): (second_stream * rms_scale(second_stream) * norm_gain_second).astype(jnp....]
  transfers between devices with their start and end apart: 8 -> 0, of which waited for: 1 -> 0; matrix products, arithmetic and copies ran while one was open for 21% -> 0% of each run, Pallas kernels for 55% -> 0%
where the time goes in v1:
time: 107 us; the launch traced here: 106 us
  Pallas kernels  106 us (99%)
    pallas_call x1, Pallas kernels, fused_shards(): pl.pallas_call(functools.partial(layer_kernel, chips, tuple(scratch)), ou...  104 us

profile of v1, /device:TPU:0, one launch (start us, length us, event | category | flops | bytes accessed | tf_op | source)
XLA Modules:
  0.0 106.4 jit_solution(12097962325548712664)
XLA Ops:
  0.6 104.2 %layer.1 = (bf16[16,2048]{1,0:T(8,128)(2,1)}, bf16[16,128]{1,0:T(8,128)(2,1)}, bf16[16,128]{1,0:T(8,128)(2,1)}) custom-call(s32[16]{0:T(128)} %lens_ref.1, f32[32]{0:T(128)} %bias_ref.1, bf16[16,2048]{1,0:T(8,128)(2,1)} %tokens_ref.1, f32[1,2048]{1,0:T(1,128)} %bitcast.18, f32[1,2048]{1,0:T(1,128)} %bitcast.19, f32[1,2048]{1,0:T(1,128)} %bitcast.20, ...), custom_call_target="tpu_custom_call" | custom-call | tf_op jit(solution)/shard_map/layer/pallas_call | solution.py:1158
  104.9 1.5 %results.1 = (bf16[16,2048]{1,0:T(8,128)(2,1)}, bf16[16,128]{1,0:T(8,128)(2,1)}, bf16[16,128]{1,0:T(8,128)(2,1)}) custom-call(bf16[16,2048]{1,0:T(8,128)(2,1)} %get-tuple-element.6.a_ref, bf16[16,128]{1,0:T(8,128)(2,1)} %get-tuple-element.7.b_ref, bf16[16,128]{1,0:T(8,128)(2,1)} %get-tuple-element.8.c_ref), custom_call_target="tpu_custom_call" | custom-call | tf_op jit(solution)/shard_map/results/pallas_call | solution.py:1174
